TPU v7x, 256 devices: a whole 4x4x8 slice. The times are simulated.
256 devices in a mesh: rep: 2 (over z_hi), fs: 16 (over z_lo, y), tp: 8 (over x, core).
Axes of the slice: x: 4, y: 4, z: 8 (z_hi: 2, z_lo: 4; z = z_hi * 4 + z_lo), core: 2. Of those that a mesh axis runs over, the one named last changes fastest.
Arguments:
- tokens: bfloat16 [65536, 2048], P(('rep', 'fs', 'tp')), may hold values from -6 to 6
- norm_gain: float32 [2048], replicated, may hold values from 0.1 to 1.9
- gate_weight: float32 [2048, 5120], P('fs', 'tp'), may hold values from -0.125 to 0.125
- gate_scale: float32 [5120], P('tp'), may hold values from 0.1 to 1.9
- up_weight: float32 [2048, 5120], P('fs', 'tp'), may hold values from -0.125 to 0.125
- up_scale: float32 [5120], P('tp'), may hold values from 0.1 to 1.9
- down_weight: float32 [5120, 2048], P('tp', 'fs'), may hold values from -0.078125 to 0.078125
- down_scale: float32 [2048], replicated, may hold values from 0.1 to 1.9
Outputs:
- mixed: bfloat16 [65536, 2048], P(('rep', 'fs', 'tp'))
All inputs are finite; a program needn't handle non-finite values.
Results may differ from a plain program's by a relative error of at most 0.013.
Values may be sent and summed in bfloat16 or wider, within the bound.
No kernel may reach another device: no remote copies, remote signals or barrier semaphores. Data moves between devices by JAX's collectives and lax.ppermute only.
A program may use at most 128 MiB of HBM per device.

v0:
```python
import jax
import jax.numpy as jnp
from jax import lax
from jax.sharding import PartitionSpec as P

EPS_VALUE = 1e-06


def rows_first(arrays, axis, dims):
    turned = [jnp.moveaxis(a, dim, 0) for a, dim in zip(arrays, dims)]
    both = jnp.concatenate([t.reshape(len(t), -1) for t in turned], axis=1)
    whole, at, outs = (lax.all_gather(both, axis, axis=0, tiled=True), 0, [])
    for t, dim in zip(turned, dims):
        piece = whole[:, at : at + t[0].size].reshape(-1, *t.shape[1:])
        outs.append(jnp.moveaxis(piece, 0, dim))
        at += t[0].size
    return tuple(outs)


def joined_along(parts, dim):
    parts = jnp.moveaxis(parts, 0, dim)
    shape = parts.shape
    return parts.reshape(*shape[:dim], shape[dim] * shape[dim + 1], *shape[dim + 2 :])


def piecewise(shard, axis, dim, apply, out_dim):
    peers, rows = (lax.axis_size(axis), shard.shape[dim])
    count = 2 if rows % 2 == 0 else 1
    outs, length = ([], rows // count)
    for k in range(count):
        piece = lax.slice_in_dim(shard, k * length, (k + 1) * length, axis=dim)
        starts = jnp.arange(peers) * rows + k * length
        outs.append(jax.vmap(apply)(lax.all_gather(piece, axis), starts))
    return joined_along(jnp.concatenate(outs, axis=out_dim + 1), out_dim)


def normalize(token_rows, norm_gain):
    values = token_rows.astype(jnp.float32)
    inverse = lax.rsqrt(jnp.mean(values * values, axis=-1, keepdims=True) + EPS_VALUE)
    return (values * inverse * norm_gain).astype(jnp.bfloat16)


def body(tokens, norm_gain, gate_weight, gate_scale, up_weight, up_scale, down_weight, down_scale):
    normed = normalize(tokens, norm_gain)
    gate_bf = gate_weight.astype(jnp.bfloat16)
    up_bf = up_weight.astype(jnp.bfloat16)
    down_bf = down_weight.astype(jnp.bfloat16)
    gate_full, up_full, down_full = rows_first((gate_bf, up_bf, down_bf), "fs", (0, 0, 1))

    def expand(slab_rows, offset):
        gate_pre = jnp.dot(slab_rows, gate_full, preferred_element_type=jnp.float32) * gate_scale
        up_pre = jnp.dot(slab_rows, up_full, preferred_element_type=jnp.float32) * up_scale
        return (jax.nn.silu(gate_pre) * up_pre).astype(jnp.bfloat16)

    hidden = piecewise(normed, "tp", 0, expand, 0)
    partial_value = (
        jnp.dot(hidden, down_full, preferred_element_type=jnp.float32) * down_scale
    ).astype(jnp.bfloat16)
    partial_value = lax.optimization_barrier(partial_value)
    return lax.psum_scatter(
        partial_value.astype(jnp.float32).astype(jnp.bfloat16),
        "tp",
        scatter_dimension=0,
        tiled=True,
    )


def solution(mesh):
    return jax.shard_map(
        body,
        mesh=mesh,
        in_specs=(
            P(("rep", "fs", "tp"), None),
            P(),
            P("fs", "tp"),
            P("tp"),
            P("fs", "tp"),
            P("tp"),
            P("tp", "fs"),
            P(),
        ),
        out_specs=P(("rep", "fs", "tp"), None),
        check_vma=False,
    )
```

profile of v0, /device:TPU:1, one launch (start us, length us, event | category | flops | bytes accessed | tf_op | source)
XLA Modules:
  0.0 268.4 jit_solution(17899285519200331253)
XLA Ops:
  6.5 0.0 all-gather.8.cloned.1.call-start
  6.5 1.5 fusion.1
  8.1 0.0 copy-start.1
  8.1 0.0 copy-start.2
  8.1 1.6 fusion.3
  9.7 1.1 fusion.8
  10.8 0.0 all-gather.8.cloned.1.call-update
  10.8 0.0 all-gather.6.cloned.1.call-start
  10.9 0.0 copy-done
  10.9 0.2 copy.9
  11.1 0.8 pad_maximum_fusion.1
  12.0 0.0 all-gather.6.cloned.1.call-update
  12.0 0.0 all-gather.10.cloned.1.call-start
  12.0 0.7 all-gather.10.cloned.1.call-update
  12.7 0.0 reduce-scatter.2.cloned.1.call-start
  12.8 37.0 %all-gather.8.cloned.1.call-done = bf16[1024,2048]{1,0:T(8,128)(2,1)} async-done(((bf16[128,2048]{1,0:T(8,128)(2,1)}), bf16[1024,2048]{1,0:T(8,128)(2,1)}) %all-gather.8.cloned.1.call-update) | async-done | bytes 4194320 | tf_op jit(solution)/shard_map/all_gather | solution.py:33
  49.8 95.3 %all-gather.6.cloned.1.call-done = bf16[2048,1920]{1,0:T(8,128)(2,1)} async-done(((bf16[128,1920]{1,0:T(8,128)(2,1)}), bf16[2048,1920]{1,0:T(8,128)(2,1)}) %all-gather.6.cloned.1.call-update) | async-done | bytes 7864336 | tf_op jit(solution)/shard_map/all_gather | solution.py:12
  145.1 6.0 %fusion.5 = f32[8,128,640]{2,1,0:T(8,128)S(1)} fusion(bf16[8,128,2048]{2,1,0:T(8,128)(2,1)} %bitcast.25, bf16[2048,1920]{1,0:T(8,128)(2,1)} %all-gather.6.cloned.1.call-done), kind=kOutput, calls=%fused_computation.13 | convolution fusion | flops 2684354560 | bytes 9437184 | tf_op jit(solution)/shard_map/vmap()/dot_general | solution.py:51
  151.1 33.0 %all-gather.10.cloned.1.call-done = bf16[1024,2048]{1,0:T(8,128)(2,1)} async-done(((bf16[128,2048]{1,0:T(8,128)(2,1)}), bf16[1024,2048]{1,0:T(8,128)(2,1)}) %all-gather.10.cloned.1.call-update) | async-done | bytes 4194320 | tf_op jit(solution)/shard_map/all_gather | solution.py:33
  184.1 6.1 %fusion.4 = f32[8,128,640]{2,1,0:T(8,128)S(1)} fusion(bf16[8,128,2048]{2,1,0:T(8,128)(2,1)} %bitcast.27, bf16[2048,1920]{1,0:T(8,128)(2,1)} %all-gather.6.cloned.1.call-done), kind=kOutput, calls=%fused_computation.12 | convolution fusion | flops 2684354560 | bytes 9437184 | tf_op jit(solution)/shard_map/vmap()/dot_general | solution.py:51
  190.3 0.0 copy-done.3
  190.3 0.3 copy-done.4
  190.6 0.0 copy-done.8
  190.6 3.6 %multiply_convert_fusion.2 = bf16[8,128,640]{2,1,0:T(8,128)(2,1)S(1)} fusion(f32[8,128,640]{2,1,0:T(8,128)S(1)} %fusion.5, bf16[8,128,2048]{2,1,0:T(8,128)(2,1)S(1)} %bitcast.26, bf16[2048,1920]{1,0:T(8,128)(2,1)S(1)} %copy-done.3, f32[640]{0:T(1024)S(1)} %copy-done.7, f32[640]{0:T(1024)S(1)} %copy-done.8), kind=kOutput, calls=%fused_computation.8 | convolution fusion | flops 2689597440 | bytes 10756096 | tf_op jit(solution)/shard_map/vmap()/dot_general | solution.py:52
  194.2 0.0 copy-done.5
  194.2 3.6 %multiply_convert_fusion.1 = bf16[8,128,640]{2,1,0:T(8,128)(2,1)S(1)} fusion(f32[8,128,640]{2,1,0:T(8,128)S(1)} %fusion.4, bf16[8,128,2048]{2,1,0:T(8,128)(2,1)S(1)} %bitcast.28, bf16[2048,1920]{1,0:T(8,128)(2,1)S(1)} %copy-done.3, f32[640]{0:T(1024)S(1)} %copy-done.7, f32[640]{0:T(1024)S(1)} %copy-done.8), kind=kOutput, calls=%fused_computation.7 | convolution fusion | flops 2689597440 | bytes 10756096 | tf_op jit(solution)/shard_map/vmap()/dot_general | solution.py:52
  197.9 0.0 copy-start.6
  197.9 0.2 pad_maximum_fusion
  198.1 0.5 copy-done.6
  198.6 9.1 %multiply_convert_fusion = bf16[2048,2048]{1,0:T(8,128)(2,1)} fusion(bf16[2048,640]{1,0:T(8,128)(2,1)S(1)} %bitcast.23, f32[2048]{0:T(1024)S(1)} %copy-done.6, bf16[2048,1920]{1,0:T(8,128)(2,1)S(1)} %copy-done.3), kind=kOutput, calls=%fused_computation | convolution fusion | flops 5377097728 | bytes 13639680 | tf_op jit(solution)/shard_map/dot_general | solution.py:57
  207.6 0.0 reduce-scatter.2.cloned.1.call-update
  207.7 54.2 %reduce-scatter.2.cloned.1.call-done = bf16[256,2048]{1,0:T(8,128)(2,1)} async-done(((bf16[2048,2048]{1,0:T(8,128)(2,1)}), bf16[256,2048]{1,0:T(8,128)(2,1)}) %reduce-scatter.2.cloned.1.call-update) | async-done | bytes 1048592 | tf_op jit(solution)/shard_map/reduce_scatter | solution.py:60
  (12 shorter events, 0.1 us)
Async XLA Ops:
  6.5 43.2 %all-gather.8.cloned.1.call-start = ((), (), s32[]{:S(2)}) async-start(), calls=%async_computation.3 | async-start | bytes 4718592 | tf_op jit(solution)/shard_map/all_gather | solution.py:33
  8.0 2.9 %copy-start = (f32[640,128]{1,0:T(8,128)S(1)}, f32[640,128]{1,0:T(8,128)}, u32[]{:S(2)}) copy-start(f32[640,128]{1,0:T(8,128)} %param.14) | copy-start | bytes 983044
  8.1 3.0 %copy-start.1 = (f32[128,640]{1,0:T(8,128)S(1)}, f32[128,640]{1,0:T(8,128)}, u32[]{:S(2)}) copy-start(f32[128,640]{1,0:T(8,128)} %param.10) | copy-start | bytes 983044
  8.1 3.0 %copy-start.2 = (f32[128,640]{1,0:T(8,128)S(1)}, f32[128,640]{1,0:T(8,128)}, u32[]{:S(2)}) copy-start(f32[128,640]{1,0:T(8,128)} %param.12) | copy-start | bytes 983044
  10.8 134.2 %all-gather.6.cloned.1.call-start = ((), (), s32[]{:S(2)}) async-start(), calls=%async_computation.1 | async-start | bytes 8355840 | tf_op jit(solution)/shard_map/all_gather | solution.py:12
  12.0 172.1 %all-gather.10.cloned.1.call-start = ((), (), s32[]{:S(2)}) async-start(), calls=%async_computation.4 | async-start | bytes 4718592 | tf_op jit(solution)/shard_map/all_gather | solution.py:33
  12.7 249.1 %reduce-scatter.2.cloned.1.call-start = ((), (), s32[]{:S(2)}) async-start(), calls=%async_computation.2 | async-start | bytes 9437184 | tf_op jit(solution)/shard_map/reduce_scatter | solution.py:60
  184.1 6.2 %copy-start.3 = (bf16[2048,1920]{1,0:T(8,128)(2,1)S(1)}, bf16[2048,1920]{1,0:T(8,128)(2,1)}, u32[]{:S(2)}) copy-start(bf16[2048,1920]{1,0:T(8,128)(2,1)} %all-gather.6.cloned.1.call-done) | copy-start | bytes 23592964
  184.1 6.5 %copy-start.4 = (bf16[1024,2048]{1,0:T(8,128)(2,1)S(1)}, bf16[1024,2048]{1,0:T(8,128)(2,1)}, u32[]{:S(2)}) copy-start(bf16[1024,2048]{1,0:T(8,128)(2,1)} %all-gather.8.cloned.1.call-done) | copy-start | bytes 12582916
  184.1 6.5 %copy-start.7 = (f32[640]{0:T(1024)S(1)}, f32[640]{0:T(1024)}, u32[]{:S(2)}) copy-start(f32[640]{0:T(1024)} %param.13) | copy-start | bytes 7684
  184.1 6.5 %copy-start.8 = (f32[640]{0:T(1024)S(1)}, f32[640]{0:T(1024)}, u32[]{:S(2)}) copy-start(f32[640]{0:T(1024)} %param.11) | copy-start | bytes 7684
  190.6 3.6 %copy-start.5 = (bf16[1024,2048]{1,0:T(8,128)(2,1)S(1)}, bf16[1024,2048]{1,0:T(8,128)(2,1)}, u32[]{:S(2)}) copy-start(bf16[1024,2048]{1,0:T(8,128)(2,1)} %all-gather.10.cloned.1.call-done) | copy-start | bytes 12582916
  197.9 0.7 copy-start.6
Sparse Core Ops, SparseCore 0:
  11.0 38.7 all-gather.7
  51.5 93.4 all-gather.5
  146.9 37.1 all-gather.9
  207.8 54.0 reduce-scatter.1
where the time goes:
time: 269 us; the launch traced here: 268 us
  waiting for transfers between devices  220 us (82%)
  matrix products  28.5 us (11%)
  between operations  13.3 us (5%)
  other arithmetic  4.22 us (2%)
    all_gather x1, waiting for transfers between devices, rows_first(): whole, at, outs = (lax.all_gather(both, axis, axis=0, tiled=True), 0, [])  95.3 us
    all_gather x2, waiting for transfers between devices, piecewise(): outs.append(jax.vmap(apply)(lax.all_gather(piece, axis), starts))  70 us
    reduce_scatter x1, waiting for transfers between devices, body(): lax.psum_scatter(partial_value.astype(jnp.float32).astype(jnp.bfloat16),...  54.2 us
    dot_general x2, matrix products, expand(): jnp.dot(slab_rows, gate_full, preferred_element_type=jnp.float32)  12.1 us
    dot_general x1, matrix products, body(): jnp.dot(hidden, down_full, preferred_element_type=jnp.float32) * down_scale  9.07 us
    dot_general x2, matrix products, expand(): jnp.dot(slab_rows, up_full, preferred_element_type=jnp.float32) * up_scale  7.26 us
  transfers between devices with their start and end apart: 4, of which 4 were waited for; matrix products, arithmetic and copies ran while one was open for 3% of the time, Pallas kernels for 0%

commit v1 on v0

--- a/solution.py
+++ b/solution.py
@@ -9,7 +9,13 @@
 def rows_first(arrays, axis, dims):
     turned = [jnp.moveaxis(a, dim, 0) for a, dim in zip(arrays, dims)]
     both = jnp.concatenate([t.reshape(len(t), -1) for t in turned], axis=1)
-    whole, at, outs = (lax.all_gather(both, axis, axis=0, tiled=True), 0, [])
+    whole, at, outs = (
+        jnp.concatenate(
+            lax.all_to_all(jnp.stack([both] * lax.axis_size(axis)), axis, 0, 0), axis=0
+        ),
+        0,
+        [],
+    )
     for t, dim in zip(turned, dims):
         piece = whole[:, at : at + t[0].size].reshape(-1, *t.shape[1:])
         outs.append(jnp.moveaxis(piece, 0, dim))

time: 269 us -> 292 us (1.086)
  starting transfers between devices: 0.12 us -> 9.47 us
  local copies, waits for them, and re-layouts: 2.05 us -> 8.22 us
  matrix products: 28.5 us -> 33.6 us
  waiting for transfers between devices: 220 us -> 225 us
    all_to_all x0 -> x1, waiting for transfers between devices: none -> 104 us  [rows_first(): lax.all_to_all(jnp.stack([both] * lax.axis_size(axis)), axis, 0, 0)]
    all_gather x1 -> x0, waiting for transfers between devices: 95.3 us -> none  [rows_first(): whole, at, outs = (lax.all_gather(both, axis, axis=0, tiled=True), 0, [])]
    all_gather x2, waiting for transfers between devices: 70 us -> 35.8 us  [piecewise(): outs.append(jax.vmap(apply)(lax.all_gather(piece, axis), starts))]
    reduce_scatter x1, waiting for transfers between devices: 54.2 us -> 84.5 us  [body(): lax.psum_scatter(partial_value.astype(jnp.float32).astype(jnp.bfloat16),...]
    all_to_all x0 -> x1, starting transfers between devices: none -> 9.35 us  [rows_first(): lax.all_to_all(jnp.stack([both] * lax.axis_size(axis)), axis, 0, 0)]
    another operation x0 -> x1, local copies, waits for them, and re-layouts: none -> 4.1 us  [rows_first(): jnp.stack([both] * lax.axis_size(axis))]
    dot_general x2, matrix products: 7.26 us -> 10.8 us  [expand(): jnp.dot(slab_rows, up_full, preferred_element_type=jnp.float32) * up_scale]
  transfers between devices with their start and end apart: 4 -> 4, of which waited for: 4 -> 3; matrix products, arithmetic and copies ran while one was open for 3% -> 3% of each run, Pallas kernels for 0% -> 0%
where the time goes in v1:
time: 292 us; the launch traced here: 291 us
  waiting for transfers between devices  225 us (77%)
  matrix products  33.6 us (12%)
  between operations  13.3 us (5%)
  starting transfers between devices  9.47 us (3%)
  local copies, waits for them, and re-layouts  8.22 us (3%)
    all_to_all x1, waiting for transfers between devices, rows_first(): lax.all_to_all(jnp.stack([both] * lax.axis_size(axis)), axis, 0, 0)  104 us
    reduce_scatter x1, waiting for transfers between devices, body(): lax.psum_scatter(partial_value.astype(jnp.float32).astype(jnp.bfloat16),...  84.5 us
    all_gather x2, waiting for transfers between devices, piecewise(): outs.append(jax.vmap(apply)(lax.all_gather(piece, axis), starts))  35.8 us
    dot_general x2, matrix products, expand(): jnp.dot(slab_rows, gate_full, preferred_element_type=jnp.float32)  12.1 us
    dot_general x2, matrix products, expand(): jnp.dot(slab_rows, up_full, preferred_element_type=jnp.float32) * up_scale  10.8 us
    dot_general x1, matrix products, body(): jnp.dot(hidden, down_full, preferred_element_type=jnp.float32) * down_scale  10.7 us
    all_to_all x1, starting transfers between devices, rows_first(): lax.all_to_all(jnp.stack([both] * lax.axis_size(axis)), axis, 0, 0)  9.35 us
  transfers between devices with their start and end apart: 4, of which 3 were waited for; matrix products, arithmetic and copies ran while one was open for 3% of the time, Pallas kernels for 0%

profile of v1, /device:TPU:1, one launch (start us, length us, event | category | flops | bytes accessed | tf_op | source)
XLA Modules:
  0.0 291.3 jit_solution(13983659900307279661)
XLA Ops:
  6.5 1.0 convert_bitcast_fusion
  7.5 1.1 copy.10
  8.7 1.1 copy.9
  9.8 0.3 copy.11
  10.1 4.1 %stack.2 = bf16[16,128,1920]{2,1,0:T(8,128)(2,1)} broadcast(bf16[128,1920]{1,0:T(8,128)(2,1)S(1)} %copy.11), dimensions={1,2} | broadcast | bytes 8355840 | tf_op jit(solution)/shard_map/stack | solution.py:14
  14.2 9.3 %all-to-all-start = ((bf16[16,128,1920]{2,1,0:T(8,128)(2,1)}), bf16[16,128,1920]{2,1,0:T(8,128)(2,1)}, u32[]{:S(2)}, u32[]{:S(2)}) async-start(bf16[16,128,1920]{2,1,0:T(8,128)(2,1)} %stack.2), calls=%async_computation | async-start | bytes 15728640 | tf_op jit(solution)/shard_map/all_to_all | solution.py:14
  23.6 0.0 all-gather.5.cloned.1.call-start
  23.6 0.3 fusion.1
  23.9 0.3 fusion.3
  24.2 1.1 fusion.8
  25.4 0.0 all-gather.5.cloned.1.call-update
  25.4 0.0 all-gather.7.cloned.1.call-start
  25.4 0.7 all-gather.7.cloned.1.call-update
  26.1 0.0 reduce-scatter.2.cloned.1.call-start
  26.2 35.8 %all-gather.5.cloned.1.call-done = bf16[1024,2048]{1,0:T(8,128)(2,1)} async-done(((bf16[128,2048]{1,0:T(8,128)(2,1)}), bf16[1024,2048]{1,0:T(8,128)(2,1)}) %all-gather.5.cloned.1.call-update) | async-done | bytes 4194320 | tf_op jit(solution)/shard_map/all_gather | solution.py:39
  62.0 103.8 %all-to-all-done = bf16[16,128,1920]{2,1,0:T(8,128)(2,1)} async-done(((bf16[16,128,1920]{2,1,0:T(8,128)(2,1)}), bf16[16,128,1920]{2,1,0:T(8,128)(2,1)}, u32[]{:S(2)}, u32[]{:S(2)}) %all-to-all-start) | async-done | bytes 7864352 | tf_op jit(solution)/shard_map/all_to_all | solution.py:14
  165.7 6.0 %fusion.5 = f32[8,128,640]{2,1,0:T(8,128)S(1)} fusion(bf16[8,128,2048]{2,1,0:T(8,128)(2,1)} %bitcast.24, bf16[2048,1920]{1,0:T(8,128)(2,1)} %bitcast.2), kind=kOutput, calls=%fused_computation.13 | convolution fusion | flops 2684354560 | bytes 9437184 | tf_op jit(solution)/shard_map/vmap()/dot_general | solution.py:57
  171.7 0.0 all-gather.7.cloned.1.call-done
  171.8 0.0 copy-start.5
  171.8 0.0 copy-start.6
  171.8 6.1 %fusion.4 = f32[8,128,640]{2,1,0:T(8,128)S(1)} fusion(bf16[8,128,2048]{2,1,0:T(8,128)(2,1)} %bitcast.26, bf16[2048,1920]{1,0:T(8,128)(2,1)} %bitcast.2), kind=kOutput, calls=%fused_computation.12 | convolution fusion | flops 2684354560 | bytes 9437184 | tf_op jit(solution)/shard_map/vmap()/dot_general | solution.py:57
  177.9 0.0 copy-done.2
  178.0 0.0 copy-done.5
  178.0 0.0 copy-done.6
  178.0 5.5 %multiply_convert_fusion.2 = bf16[8,128,640]{2,1,0:T(8,128)(2,1)S(1)} fusion(f32[8,128,640]{2,1,0:T(8,128)S(1)} %fusion.5, bf16[8,128,2048]{2,1,0:T(8,128)(2,1)S(1)} %bitcast.25, bf16[2048,1920]{1,0:T(8,128)(2,1)} %bitcast.2, f32[640]{0:T(1024)S(1)} %copy-done.5, f32[640]{0:T(1024)S(1)} %copy-done.6), kind=kOutput, calls=%fused_computation.8 | convolution fusion | flops 2689597440 | bytes 10753024 | tf_op jit(solution)/shard_map/vmap()/dot_general | solution.py:58
  183.5 5.3 %multiply_convert_fusion.1 = bf16[8,128,640]{2,1,0:T(8,128)(2,1)S(1)} fusion(f32[8,128,640]{2,1,0:T(8,128)S(1)} %fusion.4, bf16[8,128,2048]{2,1,0:T(8,128)(2,1)S(1)} %bitcast.27, bf16[2048,1920]{1,0:T(8,128)(2,1)} %bitcast.2, f32[640]{0:T(1024)S(1)} %copy-done.5, f32[640]{0:T(1024)S(1)} %copy-done.6), kind=kOutput, calls=%fused_computation.7 | convolution fusion | flops 2689597440 | bytes 10753024 | tf_op jit(solution)/shard_map/vmap()/dot_general | solution.py:58
  188.8 0.0 copy-start.4
  188.8 0.2 pad_maximum_fusion
  189.1 0.5 copy-done.4
  189.5 10.7 %multiply_convert_fusion = bf16[2048,2048]{1,0:T(8,128)(2,1)} fusion(bf16[2048,640]{1,0:T(8,128)(2,1)S(1)} %bitcast.23, f32[2048]{0:T(1024)S(1)} %copy-done.4, bf16[2048,1920]{1,0:T(8,128)(2,1)} %bitcast.2), kind=kOutput, calls=%fused_computation | convolution fusion | flops 5377097728 | bytes 13639680 | tf_op jit(solution)/shard_map/dot_general | solution.py:63
  200.2 0.0 reduce-scatter.2.cloned.1.call-update
  200.2 84.5 %reduce-scatter.2.cloned.1.call-done = bf16[256,2048]{1,0:T(8,128)(2,1)} async-done(((bf16[2048,2048]{1,0:T(8,128)(2,1)}), bf16[256,2048]{1,0:T(8,128)(2,1)}) %reduce-scatter.2.cloned.1.call-update) | async-done | bytes 1048592 | tf_op jit(solution)/shard_map/reduce_scatter | solution.py:66
  (9 shorter events, 0.1 us)
Async XLA Ops:
  14.2 9.4 %copy-start = (bf16[256,2048]{1,0:T(8,128)(2,1)S(1)}, bf16[256,2048]{1,0:T(8,128)(2,1)}, u32[]{:S(2)}) copy-start(bf16[256,2048]{1,0:T(8,128)(2,1)} %param.8) | copy-start | bytes 3145732
  14.2 9.7 %copy-start.1 = (f32[2048]{0:T(1024)S(1)}, f32[2048]{0:T(1024)}, u32[]{:S(2)}) copy-start(f32[2048]{0:T(1024)} %param.9) | copy-start | bytes 24580
  14.2 151.5 %all-to-all-start = ((bf16[16,128,1920]{2,1,0:T(8,128)(2,1)}), bf16[16,128,1920]{2,1,0:T(8,128)(2,1)}, u32[]{:S(2)}, u32[]{:S(2)}) async-start(bf16[16,128,1920]{2,1,0:T(8,128)(2,1)} %stack.2), calls=%async_computation | async-start | bytes 15728640 | tf_op jit(solution)/shard_map/all_to_all | solution.py:14
  23.6 38.4 %all-gather.5.cloned.1.call-start = ((), (), s32[]{:S(2)}) async-start(), calls=%async_computation.3 | async-start | bytes 4718592 | tf_op jit(solution)/shard_map/all_gather | solution.py:39
  25.4 146.4 %all-gather.7.cloned.1.call-start = ((), (), s32[]{:S(2)}) async-start(), calls=%async_computation.4 | async-start | bytes 4718592 | tf_op jit(solution)/shard_map/all_gather | solution.py:39
  26.1 258.6 %reduce-scatter.2.cloned.1.call-start = ((), (), s32[]{:S(2)}) async-start(), calls=%async_computation.2 | async-start | bytes 9437184 | tf_op jit(solution)/shard_map/reduce_scatter | solution.py:66
  171.8 6.2 %copy-start.2 = (bf16[1024,2048]{1,0:T(8,128)(2,1)S(1)}, bf16[1024,2048]{1,0:T(8,128)(2,1)}, u32[]{:S(2)}) copy-start(bf16[1024,2048]{1,0:T(8,128)(2,1)} %all-gather.5.cloned.1.call-done) | copy-start | bytes 12582916
  171.8 6.2 %copy-start.5 = (f32[640]{0:T(1024)S(1)}, f32[640]{0:T(1024)}, u32[]{:S(2)}) copy-start(f32[640]{0:T(1024)} %param.13) | copy-start | bytes 7684
  171.8 6.2 %copy-start.6 = (f32[640]{0:T(1024)S(1)}, f32[640]{0:T(1024)}, u32[]{:S(2)}) copy-start(f32[640]{0:T(1024)} %param.11) | copy-start | bytes 7684
  178.0 5.5 %copy-start.3 = (bf16[1024,2048]{1,0:T(8,128)(2,1)S(1)}, bf16[1024,2048]{1,0:T(8,128)(2,1)}, u32[]{:S(2)}) copy-start(bf16[1024,2048]{1,0:T(8,128)(2,1)} %all-gather.7.cloned.1.call-done) | copy-start | bytes 12582916
  188.8 0.7 copy-start.4
Sparse Core Ops, SparseCore 0:
  26.2 35.7 all-gather.4
  63.9 34.5 all-gather.6
  200.3 84.3 reduce-scatter.1
